TPU v7x, 32 devices: a whole 2x2x4 slice. The times are simulated.
32 devices in a mesh: grp: 2 (over y), sp: 4 (over z), tp: 4 (over x, core).
Axes of the slice: x: 2, y: 2, z: 4, core: 2. Of those that a mesh axis runs over, the one named last changes fastest.
Arguments:
- resid: bfloat16 [5120, 2048], P(('grp', 'sp'), 'tp'), parts along dimension 0, may hold values from -6 to 6
- queries: bfloat16 [5120, 2048], P(('grp', 'sp'), 'tp'), parts along dimension 0, may hold values from -150 to 150
- keys_values: bfloat16 [5120, 8, 128], P(('grp', 'sp'), 'tp'), parts along dimension 0, may hold values from -4.5 to 4.5
- sink: float32 [32], P('tp'), may hold values from 3 to 7
- out_weight: bfloat16 [2048, 2048], P('tp'), may hold values from -2.390625 to 2.390625
- norm_gain: float32 [2048], replicated, may hold values from 0.1 to 1.9
- gate_weight: bfloat16 [2048, 5632], P('sp', 'tp'), may hold values from -0.125 to 0.125
- up_weight: bfloat16 [2048, 5632], P('sp', 'tp'), may hold values from -0.125 to 0.125
- down_weight: bfloat16 [5632, 2048], P('tp', 'sp'), may hold values from -0.078125 to 0.078125
Outputs:
- mixed: bfloat16 [5120, 2048], P(('grp', 'sp'), 'tp'), parts along dimension 0
There are 2 independent parts, one for each index of `grp`. A program takes and returns all parts, laid end to end along the dimension named above; an argument that names none is the same for every part. Nothing has to cross between parts.
All inputs are finite; a program needn't handle non-finite values.
Results may differ from a plain program's by a relative error of at most 0.008.
Values may be sent and summed in bfloat16 or wider, within the bound.
A program may use at most 128 MiB of HBM per device.

v0:
```python
import jax
import jax.numpy as jnp
from jax import lax
from jax.sharding import PartitionSpec as P

HEAD_DIM = 64
WINDOW = 128
GRID_W = 64


def with_halo(cells, sides, width):
    for axis, dim in sides:
        count = lax.axis_size(axis)
        ends = count - 1
        head = lax.slice_in_dim(cells, 0, width, axis=dim)
        tail = lax.slice_in_dim(cells, cells.shape[dim] - width, cells.shape[dim], axis=dim)
        cells = jnp.concatenate(
            [
                lax.ppermute(tail, axis, [(i, (i + 1) % count) for i in range(ends)]),
                cells,
                lax.ppermute(head, axis, [((i + 1) % count, i) for i in range(ends)]),
            ],
            axis=dim,
        )
    return cells


def rotate(values, positions):
    quarter = 16
    inverse = 10000.0 ** (-jnp.arange(quarter, dtype=jnp.float32) / quarter)

    def turn(part, place):
        angle = place.astype(jnp.float32)[:, None] * inverse[None, :]
        cosine = jnp.cos(angle)[:, None, :]
        sine = jnp.sin(angle)[:, None, :]
        first, second = (part[..., :quarter], part[..., quarter:])
        return jnp.concatenate(
            [first * cosine - second * sine, second * cosine + first * sine], axis=-1
        )

    grid_row = positions // GRID_W
    grid_col = positions % GRID_W
    return jnp.concatenate(
        [turn(values[..., :32], grid_row), turn(values[..., 32:], grid_col)], axis=-1
    )


def body(
    resid, queries, keys_values, sink, out_weight, norm_gain, gate_weight, up_weight, down_weight
):
    tok = queries.shape[0]
    heads_here = queries.shape[1] // HEAD_DIM
    kv_here = keys_values.shape[1]
    group = heads_here // kv_here
    cols = resid.shape[1]
    offset = lax.axis_index("sp") * tok
    total_tokens = tok * lax.axis_size("sp")
    positions = offset + jnp.arange(tok, dtype=jnp.int32)
    rotated_q = rotate(
        queries.astype(jnp.float32).reshape(tok, heads_here, HEAD_DIM), positions
    ).astype(jnp.bfloat16)
    rotated_k = rotate(keys_values[..., :HEAD_DIM].astype(jnp.float32), positions).astype(
        jnp.bfloat16
    )
    joined = jnp.concatenate([rotated_k, keys_values[..., HEAD_DIM:]], axis=-1)
    padded = with_halo(joined, (("sp", 0),), WINDOW)
    blocks = tok // WINDOW
    key_blocks = jnp.stack(
        [padded[index * WINDOW : index * WINDOW + 3 * WINDOW] for index in range(blocks)]
    )
    grouped = rotated_q.reshape(blocks, WINDOW, kv_here, group, HEAD_DIM)
    scores = jnp.einsum(
        "nqkgd,njkd->nkgqj", grouped, key_blocks[..., :HEAD_DIM], preferred_element_type=jnp.float32
    ) * HEAD_DIM ** (-0.5)
    block_start = offset + WINDOW * jnp.arange(blocks, dtype=jnp.int32)
    query_pos = block_start[:, None] + jnp.arange(WINDOW, dtype=jnp.int32)[None, :]
    key_pos = block_start[:, None] - WINDOW + jnp.arange(3 * WINDOW, dtype=jnp.int32)[None, :]
    valid = (
        (jnp.abs(query_pos[:, :, None] - key_pos[:, None, :]) <= WINDOW)
        & (key_pos[:, None, :] >= 0)
        & (key_pos[:, None, :] < total_tokens)
    )
    scores = jnp.where(valid[:, None, None], scores, jnp.float32(-1e30))
    sink_grid = sink.reshape(kv_here, group)[None, :, :, None]
    top = jnp.maximum(jnp.max(scores, axis=-1), sink_grid)
    expo = jnp.exp(scores - top[..., None])
    denom = jnp.sum(expo, axis=-1) + jnp.exp(sink_grid - top)
    probs = (expo / denom[..., None]).astype(jnp.bfloat16)
    attended = jnp.einsum(
        "nkgqj,njkd->nqkgd", probs, key_blocks[..., HEAD_DIM:], preferred_element_type=jnp.float32
    )
    attended = attended.astype(jnp.bfloat16).reshape(tok, heads_here * HEAD_DIM)
    attn_rows, resid_rows = (
        lax.all_to_all(attended, "tp", split_axis=0, concat_axis=1, tiled=True),
        lax.all_to_all(resid, "tp", split_axis=0, concat_axis=1, tiled=True),
    )
    whole_out = lax.all_gather(out_weight, "tp", axis=0, tiled=True)
    stream_part = (
        resid_rows.astype(jnp.float32)
        + jnp.dot(attn_rows, whole_out, preferred_element_type=jnp.float32)
    ).astype(jnp.bfloat16)
    stream = lax.all_gather(stream_part, "tp", axis=0, tiled=True)
    stream_cols = lax.dynamic_slice_in_dim(stream, lax.axis_index("tp") * cols, cols, 1)
    widened = stream.astype(jnp.float32)
    normed = (
        widened * lax.rsqrt(jnp.mean(widened * widened, axis=-1, keepdims=True) + 1e-06) * norm_gain
    ).astype(jnp.bfloat16)
    gate = jnp.dot(
        normed,
        lax.all_gather(gate_weight, "sp", axis=0, tiled=True),
        preferred_element_type=jnp.float32,
    )
    up = jnp.dot(
        normed,
        lax.all_gather(up_weight, "sp", axis=0, tiled=True),
        preferred_element_type=jnp.float32,
    )
    hidden = (jax.nn.silu(gate) * up).astype(jnp.bfloat16)
    terms = jnp.dot(
        hidden,
        lax.all_gather(down_weight, "sp", axis=1, tiled=True),
        preferred_element_type=jnp.float32,
    )
    summed = lax.psum_scatter(
        terms.astype(jnp.bfloat16), "tp", scatter_dimension=1, tiled=True
    ).astype(jnp.float32)
    return (stream_cols.astype(jnp.float32) + summed).astype(jnp.bfloat16)


def solution(mesh):
    return jax.shard_map(
        body,
        mesh=mesh,
        in_specs=(
            P(("grp", "sp"), "tp"),
            P(("grp", "sp"), "tp"),
            P(("grp", "sp"), "tp", None),
            P("tp"),
            P("tp", None),
            P(),
            P("sp", "tp"),
            P("sp", "tp"),
            P("tp", "sp"),
        ),
        out_specs=P(("grp", "sp"), "tp"),
        check_vma=False,
    )
```

profile of v0, /device:TPU:0, one launch (start us, length us, event | category | flops | bytes accessed | tf_op | source)
XLA Modules:
  0.0 493.6 jit_solution(14125125992527969314)
XLA Ops:
  6.5 0.7 all-gather.6.cloned.1.call-update
  7.3 1.7 fusion.49
  8.9 0.2 copy.43
  9.2 0.2 copy.44
  9.4 0.4 multiply_cosine_fusion.1
  9.9 5.0 %collective-permute-start = (bf16[128,2,128]{0,2,1:T(8,128)(2,1)S(1)}, bf16[128,2,128]{0,2,1:T(8,128)(2,1)S(1)}, u32[]{:S(2)}, u32[]{:S(2)}) collective-permute-start(bf16[128,2,128]{0,2,1:T(8,128)(2,1)S(1)} %get-tuple-element.12), channel_id=1, source_target_pairs={{0,4},{4,8},{8,12},{1,5},{5,9},{9,13},{2,6},{6,10},{10,14},{3,7},{... | collective-permute-start | bytes 196616 | tf_op jit(solution)/shard_map/ppermute | solution.py:19
  14.9 1.3 collective-permute-start.1
  16.2 3.5 all-to-all-start
  19.7 0.3 copy.32
  20.1 0.1 convert.39
  20.2 0.1 iota_add_fusion.1
  20.2 0.1 fusion.36
  20.3 0.1 iota_add_fusion
  20.4 0.2 subtract_convert_fusion.1
  20.6 1.2 fusion.11
  21.8 0.2 concatenate.29
  22.0 0.2 concatenate.30
  22.2 0.2 concatenate.31
  22.5 0.2 concatenate.32
  22.7 0.1 max.17
  23.0 1.3 fusion.1
  24.3 0.1 broadcast_maximum_fusion
  24.4 1.9 fusion
  26.3 0.1 exponential_add_fusion
  26.4 2.3 fusion.9
  28.7 1.6 copy.38
  30.3 1.6 all_to_all.26
  31.9 5.0 %all-to-all-done = bf16[4,160,512]{2,1,0:T(8,128)(2,1)S(1)} async-done(((bf16[4,160,512]{2,1,0:T(8,128)(2,1)}), bf16[4,160,512]{2,1,0:T(8,128)(2,1)S(1)}, u32[]{:S(2)}, u32[]{:S(2)}) %all-to-all-start) | async-done | bytes 655392 | tf_op jit(solution)/shard_map/all_to_all | solution.py:95
  36.9 3.5 all-to-all-start.1
  40.5 0.2 convert_bitcast_fusion
  40.6 0.1 copy.45
  40.8 17.3 %all-to-all-done.1 = bf16[4,160,512]{2,1,0:T(8,128)(2,1)S(1)} async-done(((bf16[4,160,512]{2,1,0:T(8,128)(2,1)}), bf16[4,160,512]{2,1,0:T(8,128)(2,1)S(1)}, u32[]{:S(2)}, u32[]{:S(2)}) %all-to-all-start.1) | async-done | bytes 655392 | tf_op jit(solution)/shard_map/all_to_all | solution.py:94
  58.0 0.1 copy.46
  58.1 25.6 %all-gather.6.cloned.1.call-done = bf16[2048,2048]{1,0:T(8,128)(2,1)} async-done(((bf16[512,2048]{1,0:T(8,128)(2,1)}), bf16[2048,2048]{1,0:T(8,128)(2,1)}) %all-gather.6.cloned.1.call-update) | async-done | bytes 8388624 | tf_op jit(solution)/shard_map/all_gather | solution.py:97
  83.7 5.7 %fusion.7 = bf16[160,2048]{1,0:T(8,128)(2,1)} fusion(f32[160,2048]{1,0:T(8,128)S(1)} %bitcast.70, bf16[160,2048]{1,0:T(8,128)(2,1)S(1)} %bitcast.71, bf16[2048,2048]{1,0:T(8,128)(2,1)} %all-gather.6.cloned.1.call-done), kind=kOutput, calls=%fused_computation.15 | convolution fusion | flops 1342832640 | bytes 11010048 | tf_op jit(solution)/shard_map/dot_general | solution.py:100
  89.5 0.7 all-gather.10.cloned.1.call-update
  90.2 0.5 all-gather.12.cloned.1.call-update
  90.8 0.5 all-gather.14.cloned.1.call-update
  91.3 0.2 reduce-scatter.2.cloned.1.call-start
  91.6 23.8 %all-gather.8.cloned.1.call-done = bf16[640,2048]{1,0:T(8,128)(2,1)} async-done(((bf16[160,2048]{1,0:T(8,128)(2,1)}), bf16[640,2048]{1,0:T(8,128)(2,1)}) %all-gather.8.cloned.1.call-update) | async-done | bytes 2621456 | tf_op jit(solution)/shard_map/all_gather | solution.py:102
  115.4 2.3 fusion.2
  117.8 106.0 %all-gather.10.cloned.1.call-done = bf16[2048,1408]{1,0:T(8,128)(2,1)} async-done(((bf16[512,1408]{1,0:T(8,128)(2,1)}), bf16[2048,1408]{1,0:T(8,128)(2,1)}) %all-gather.10.cloned.1.call-update) | async-done | bytes 5767184 | tf_op jit(solution)/shard_map/all_gather | solution.py:110
  223.7 9.5 %fusion.14 = f32[640,1408]{1,0:T(8,128)} fusion(bf16[2048,1408]{1,0:T(8,128)(2,1)} %all-gather.10.cloned.1.call-done, bf16[640,2048]{1,0:T(8,128)(2,1)} %all-gather.8.cloned.1.call-done, f32[2048]{0:T(1024)S(1)} %copy-done.2, f32[640]{0:T(1024)S(1)} %add_rsqrt_fusion), kind=kOutput, calls=%fused_computation.23 | convolution fusion | flops 3696230400 | bytes 12003840 | tf_op jit(solution)/shard_map/dot_general | solution.py:108
  233.2 96.9 %all-gather.12.cloned.1.call-done = bf16[2048,1408]{1,0:T(8,128)(2,1)} async-done(((bf16[512,1408]{1,0:T(8,128)(2,1)}), bf16[2048,1408]{1,0:T(8,128)(2,1)}) %all-gather.12.cloned.1.call-update) | async-done | bytes 5767184 | tf_op jit(solution)/shard_map/all_gather | solution.py:115
  330.1 106.4 %all-gather.14.cloned.1.call-done = bf16[1408,2048]{1,0:T(8,128)(2,1)} async-done(((bf16[1408,512]{1,0:T(8,128)(2,1)}), bf16[1408,2048]{1,0:T(8,128)(2,1)}) %all-gather.14.cloned.1.call-update) | async-done | bytes 5767184 | tf_op jit(solution)/shard_map/all_gather | solution.py:121
  436.5 15.3 %convolution_convert_fusion = bf16[640,2048]{1,0:T(8,128)(2,1)} fusion(bf16[1408,2048]{1,0:T(8,128)(2,1)} %all-gather.14.cloned.1.call-done, bf16[2048,1408]{1,0:T(8,128)(2,1)} %all-gather.12.cloned.1.call-done, f32[640,1408]{1,0:T(8,128)} %fusion.14, bf16[640,2048]{1,0:T(8,128)(2,1)S(1)} %copy-done, f32[2048]{0:T(1024)S(1)} %copy-done.2, ...), kind=kOutput, calls=%fused_computation.13 | convolution fusion | flops 7393935360 | bytes 20392448 | tf_op jit(solution)/shard_map/dot_general | solution.py:119
  451.9 32.8 %reduce-scatter.2.cloned.1.call-done = bf16[640,512]{1,0:T(8,128)(2,1)} async-done(((bf16[640,2048]{1,0:T(8,128)(2,1)}), bf16[640,512]{1,0:T(8,128)(2,1)}) %reduce-scatter.2.cloned.1.call-update) | async-done | bytes 655376 | tf_op jit(solution)/shard_map/reduce_scatter | solution.py:124
  484.7 2.1 add_convert_fusion
  (37 shorter events, 0.7 us)
Async XLA Ops:
  6.5 13.2 %copy-start.1 = (bf16[640,512]{1,0:T(8,128)(2,1)S(1)}, bf16[640,512]{1,0:T(8,128)(2,1)}, u32[]{:S(2)}) copy-start(bf16[640,512]{1,0:T(8,128)(2,1)} %param.10) | copy-start | bytes 1966084
  6.5 77.1 %all-gather.6.cloned.1.call-start = ((), (), s32[]{:S(2)}) async-start(), calls=%async_computation.3 | async-start | bytes 10485760 | tf_op jit(solution)/shard_map/all_gather | solution.py:97
  9.9 12.9 %collective-permute-start = (bf16[128,2,128]{0,2,1:T(8,128)(2,1)S(1)}, bf16[128,2,128]{0,2,1:T(8,128)(2,1)S(1)}, u32[]{:S(2)}, u32[]{:S(2)}) collective-permute-start(bf16[128,2,128]{0,2,1:T(8,128)(2,1)S(1)} %get-tuple-element.12), channel_id=1, source_target_pairs={{0,4},{4,8},{8,12},{1,5},{5,9},{9,13},{2,6},{6,10},{10,14},{3,7},{... | collective-permute-start | bytes 196616 | tf_op jit(solution)/shard_map/ppermute | solution.py:19
  14.9 8.1 %collective-permute-start.1 = (bf16[128,2,128]{0,2,1:T(8,128)(2,1)S(1)}, bf16[128,2,128]{0,2,1:T(8,128)(2,1)S(1)}, u32[]{:S(2)}, u32[]{:S(2)}) collective-permute-start(bf16[128,2,128]{0,2,1:T(8,128)(2,1)S(1)} %get-tuple-element.11), channel_id=1, source_target_pairs={{4,0},{8,4},{12,8},{5,1},{9,5},{13,9},{6,2},{10,6},{14,10},{7,3},{... | collective-permute-start | bytes 196616 | tf_op jit(solution)/shard_map/ppermute | solution.py:21
  16.2 20.7 %all-to-all-start = ((bf16[4,160,512]{2,1,0:T(8,128)(2,1)}), bf16[4,160,512]{2,1,0:T(8,128)(2,1)S(1)}, u32[]{:S(2)}, u32[]{:S(2)}) async-start(bf16[4,160,512]{2,1,0:T(8,128)(2,1)} %bitcast), calls=%async_computation | async-start | bytes 1310720 | tf_op jit(solution)/shard_map/all_to_all | solution.py:95
  20.0 2.7 copy-start.3
  36.9 21.1 %all-to-all-start.1 = ((bf16[4,160,512]{2,1,0:T(8,128)(2,1)}), bf16[4,160,512]{2,1,0:T(8,128)(2,1)S(1)}, u32[]{:S(2)}, u32[]{:S(2)}) async-start(bf16[4,160,512]{2,1,0:T(8,128)(2,1)} %all_to_all.26), calls=%async_computation.1 | async-start | bytes 1310720 | tf_op jit(solution)/shard_map/all_to_all | solution.py:94
  40.4 75.0 %all-gather.8.cloned.1.call-start = ((), (), s32[]{:S(2)}) async-start(), calls=%async_computation.4 | async-start | bytes 3276800 | tf_op jit(solution)/shard_map/all_gather | solution.py:102
  89.4 134.3 %copy-start.2 = (f32[2048]{0:T(1024)S(1)}, f32[2048]{0:T(1024)}, u32[]{:S(2)}) copy-start(f32[2048]{0:T(1024)} %param.14) | copy-start | bytes 24580
  89.4 134.3 %all-gather.10.cloned.1.call-start = ((), (), s32[]{:S(2)}) async-start(), calls=%async_computation.5 | async-start | bytes 7208960 | tf_op jit(solution)/shard_map/all_gather | solution.py:110
  90.2 239.9 %all-gather.12.cloned.1.call-start = ((), (), s32[]{:S(2)}) async-start(), calls=%async_computation.6 | async-start | bytes 7208960 | tf_op jit(solution)/shard_map/all_gather | solution.py:115
  90.8 345.8 %all-gather.14.cloned.1.call-start = ((), (), s32[]{:S(2)}) async-start(), calls=%async_computation.7 | async-start | bytes 7208960 | tf_op jit(solution)/shard_map/all_gather | solution.py:121
  91.3 393.3 %reduce-scatter.2.cloned.1.call-start = ((), (), s32[]{:S(2)}) async-start(), calls=%async_computation.8 | async-start | bytes 3276800 | tf_op jit(solution)/shard_map/reduce_scatter | solution.py:124
  117.7 318.8 %copy-start = (bf16[640,2048]{1,0:T(8,128)(2,1)S(1)}, bf16[640,2048]{1,0:T(8,128)(2,1)}, u32[]{:S(2)}) copy-start(bf16[640,2048]{1,0:T(8,128)(2,1)} %all-gather.8.cloned.1.call-done) | copy-start | bytes 7864324
Sparse Core Ops, SparseCore 0:
  8.9 74.7 all-gather.5
  89.6 25.8 all-gather.7
  117.0 106.6 all-gather.9
  225.1 104.9 all-gather.11
  331.5 104.9 all-gather.13
  452.0 32.6 reduce-scatter.1
where the time goes:
time: 494 us
  waiting for transfers between devices  416 us (84%)
  matrix products  34.2 us (7%)
  between operations  13.8 us (3%)
  starting transfers between devices  13.6 us (3%)
  other arithmetic  8.95 us (2%)
  local copies, waits for them, and re-layouts  6.91 us (1%)
    all_gather x1, waiting for transfers between devices, body(): lax.all_gather(down_weight, 'sp', axis=1, tiled=True)  106 us
    all_gather x1, waiting for transfers between devices, body(): lax.all_gather(gate_weight, 'sp', axis=0, tiled=True)  106 us
    all_gather x1, waiting for transfers between devices, body(): lax.all_gather(up_weight, 'sp', axis=0, tiled=True)  96.9 us
    reduce_scatter x1, waiting for transfers between devices, body(): lax.psum_scatter(terms.astype(jnp.bfloat16), 'tp', scatter_dimension=1, t...  32.8 us
    all_gather x1, waiting for transfers between devices, body(): whole_out = lax.all_gather(out_weight, 'tp', axis=0, tiled=True)  25.6 us
    all_gather x1, waiting for transfers between devices, body(): stream = lax.all_gather(stream_part, 'tp', axis=0, tiled=True)  23.8 us
    all_to_all x1, waiting for transfers between devices, body(): lax.all_to_all(attended, 'tp', split_axis=0, concat_axis=1, tiled=True)  17.3 us
    dot_general x1, matrix products, body(): jnp.dot(hidden, lax.all_gather(down_weight, 'sp', axis=1, tiled=True), pr...  15.3 us
  transfers between devices with their start and end apart: 10, of which 8 were waited for; matrix products, arithmetic and copies ran while one was open for 5% of the time, Pallas kernels for 0%

commit v1 on v0

--- a/solution.py
+++ b/solution.py
@@ -116,10 +116,11 @@
         preferred_element_type=jnp.float32,
     )
     hidden = (jax.nn.silu(gate) * up).astype(jnp.bfloat16)
+    _cover_series_all = lambda my_data, shard_axis: jnp.concatenate(
+        lax.all_gather(my_data, axis_name=shard_axis), axis=1
+    )
     terms = jnp.dot(
-        hidden,
-        lax.all_gather(down_weight, "sp", axis=1, tiled=True),
-        preferred_element_type=jnp.float32,
+        hidden, _cover_series_all(down_weight, shard_axis="sp"), preferred_element_type=jnp.float32
     )
     summed = lax.psum_scatter(
         terms.astype(jnp.bfloat16), "tp", scatter_dimension=1, tiled=True

time: 494 us -> 490 us (level)
  waiting for transfers between devices: 416 us -> 404 us
  local copies, waits for them, and re-layouts: 6.91 us -> 14.3 us
    reshape x0 -> x1, local copies, waits for them, and re-layouts: none -> 8.42 us  [body(): jnp.concatenate(lax.all_gather(my_data, axis_name=shard_axis), axis=1)]
    all_gather x1, waiting for transfers between devices: 23.8 us -> 17 us  [body(): stream = lax.all_gather(stream_part, 'tp', axis=0, tiled=True)]
  transfers between devices with their start and end apart: 10 -> 10, of which waited for: 8 -> 8; matrix products, arithmetic and copies ran while one was open for 5% -> 8% of each run, Pallas kernels for 0% -> 0%
where the time goes in v1:
time: 490 us; the launch traced here: 489 us
  waiting for transfers between devices  404 us (82%)
  matrix products  34.2 us (7%)
  local copies, waits for them, and re-layouts  14.3 us (3%)
  between operations  13.8 us (3%)
  starting transfers between devices  13.6 us (3%)
  other arithmetic  8.98 us (2%)
    all_gather x1, waiting for transfers between devices, body(): lax.all_gather(gate_weight, 'sp', axis=0, tiled=True)  106 us
    all_gather x1, waiting for transfers between devices, body(): lax.all_gather(my_data, axis_name=shard_axis)  102 us
    all_gather x1, waiting for transfers between devices, body(): lax.all_gather(up_weight, 'sp', axis=0, tiled=True)  96.8 us
    reduce_scatter x1, waiting for transfers between devices, body(): lax.psum_scatter(terms.astype(jnp.bfloat16), 'tp', scatter_dimension=1, t...  32.8 us
    all_gather x1, waiting for transfers between devices, body(): whole_out = lax.all_gather(out_weight, 'tp', axis=0, tiled=True)  25.6 us
    all_to_all x1, waiting for transfers between devices, body(): lax.all_to_all(attended, 'tp', split_axis=0, concat_axis=1, tiled=True)  17.3 us
    all_gather x1, waiting for transfers between devices, body(): stream = lax.all_gather(stream_part, 'tp', axis=0, tiled=True)  17 us
    dot_general x1, matrix products, body(): jnp.dot(hidden, _cover_series_all(down_weight, shard_axis='sp'), preferre...  15.3 us
  transfers between devices with their start and end apart: 10, of which 8 were waited for; matrix products, arithmetic and copies ran while one was open for 8% of the time, Pallas kernels for 0%

profile of v1, /device:TPU:0, one launch (start us, length us, event | category | flops | bytes accessed | tf_op | source)
XLA Modules:
  0.0 489.2 jit_solution(13088630771603515031)
XLA Ops:
  6.5 0.7 all-gather.7.cloned.1.call-update
  7.3 0.7 all-gather.15.cloned.1.call-update
  8.0 0.6 fusion.49
  8.6 0.2 copy.56
  8.9 0.2 copy.57
  9.1 0.4 multiply_cosine_fusion.1
  9.6 5.0 %collective-permute-start = (bf16[128,2,128]{0,2,1:T(8,128)(2,1)S(1)}, bf16[128,2,128]{0,2,1:T(8,128)(2,1)S(1)}, u32[]{:S(2)}, u32[]{:S(2)}) collective-permute-start(bf16[128,2,128]{0,2,1:T(8,128)(2,1)S(1)} %get-tuple-element.12), channel_id=1, source_target_pairs={{0,4},{4,8},{8,12},{1,5},{5,9},{9,13},{2,6},{6,10},{10,14},{3,7},{... | collective-permute-start | bytes 196616 | tf_op jit(solution)/shard_map/ppermute | solution.py:19
  14.6 1.3 collective-permute-start.1
  15.9 3.5 all-to-all-start
  19.4 0.3 copy.44
  19.8 0.1 convert.39
  19.9 0.1 iota_add_fusion.1
  19.9 0.1 fusion.36
  20.0 0.1 iota_add_fusion
  20.1 0.2 subtract_convert_fusion.1
  20.3 1.2 fusion.11
  21.5 0.2 concatenate.29
  21.7 0.2 concatenate.30
  21.9 0.2 concatenate.31
  22.2 0.2 concatenate.32
  22.4 0.1 max.17
  22.7 1.3 fusion.1
  24.0 0.1 broadcast_maximum_fusion
  24.1 1.9 fusion
  26.0 0.1 exponential_add_fusion
  26.1 2.3 fusion.9
  28.4 1.6 copy.50
  30.1 1.6 all_to_all.26
  31.7 4.9 all-to-all-done
  36.6 3.5 all-to-all-start.1
  40.1 0.2 convert_bitcast_fusion
  40.3 0.1 copy.58
  40.4 17.3 %all-to-all-done.1 = bf16[4,160,512]{2,1,0:T(8,128)(2,1)S(1)} async-done(((bf16[4,160,512]{2,1,0:T(8,128)(2,1)}), bf16[4,160,512]{2,1,0:T(8,128)(2,1)S(1)}, u32[]{:S(2)}, u32[]{:S(2)}) %all-to-all-start.1) | async-done | bytes 655392 | tf_op jit(solution)/shard_map/all_to_all | solution.py:94
  57.8 25.6 %all-gather.7.cloned.1.call-done = bf16[2048,2048]{1,0:T(8,128)(2,1)} async-done(((bf16[512,2048]{1,0:T(8,128)(2,1)}), bf16[2048,2048]{1,0:T(8,128)(2,1)}) %all-gather.7.cloned.1.call-update) | async-done | bytes 8388624 | tf_op jit(solution)/shard_map/all_gather | solution.py:97
  83.4 5.8 %fusion.7 = bf16[160,2048]{1,0:T(8,128)(2,1)} fusion(f32[160,2048]{1,0:T(8,128)S(1)} %bitcast.76, bf16[160,2048]{1,0:T(8,128)(2,1)S(1)} %bitcast.77, bf16[2048,2048]{1,0:T(8,128)(2,1)} %all-gather.7.cloned.1.call-done), kind=kOutput, calls=%fused_computation.15 | convolution fusion | flops 1342832640 | bytes 11010048 | tf_op jit(solution)/shard_map/dot_general | solution.py:100
  89.2 0.5 all-gather.11.cloned.1.call-update
  89.8 0.5 all-gather.13.cloned.1.call-update
  90.3 0.2 reduce-scatter.2.cloned.1.call-start
  90.5 101.7 %all-gather.15.cloned.1.call-done = bf16[5632,512]{1,0:T(8,128)(2,1)} async-done(((bf16[1408,512]{1,0:T(8,128)(2,1)}), bf16[5632,512]{1,0:T(8,128)(2,1)}) %all-gather.15.cloned.1.call-update) | async-done | bytes 5767184 | tf_op jit(solution)/shard_map/all_gather | solution.py:120
  192.2 8.4 %copy.52 = bf16[1408,4,512]{0,2,1:T(8,128)(2,1)} copy(bf16[1408,4,512]{2,0,1:T(8,128)(2,1)} %bitcast.74) | data formatting | bytes 11534336 | tf_op jit(solution)/shard_map/reshape | solution.py:119
  200.7 17.0 %all-gather.9.cloned.1.call-done = bf16[640,2048]{1,0:T(8,128)(2,1)} async-done(((bf16[160,2048]{1,0:T(8,128)(2,1)}), bf16[640,2048]{1,0:T(8,128)(2,1)}) %all-gather.9.cloned.1.call-update) | async-done | bytes 2621456 | tf_op jit(solution)/shard_map/all_gather | solution.py:102
  217.6 2.3 fusion.2
  220.0 105.8 %all-gather.11.cloned.1.call-done = bf16[2048,1408]{1,0:T(8,128)(2,1)} async-done(((bf16[512,1408]{1,0:T(8,128)(2,1)}), bf16[2048,1408]{1,0:T(8,128)(2,1)}) %all-gather.11.cloned.1.call-update) | async-done | bytes 5767184 | tf_op jit(solution)/shard_map/all_gather | solution.py:110
  325.8 9.6 %fusion.14 = f32[640,1408]{1,0:T(8,128)} fusion(bf16[2048,1408]{1,0:T(8,128)(2,1)} %all-gather.11.cloned.1.call-done, bf16[640,2048]{1,0:T(8,128)(2,1)} %all-gather.9.cloned.1.call-done, f32[2048]{0:T(1024)S(1)} %copy-done.3, f32[640]{0:T(1024)S(1)} %add_rsqrt_fusion), kind=kOutput, calls=%fused_computation.23 | convolution fusion | flops 3696230400 | bytes 12003840 | tf_op jit(solution)/shard_map/dot_general | solution.py:108
  335.3 96.8 %all-gather.13.cloned.1.call-done = bf16[2048,1408]{1,0:T(8,128)(2,1)} async-done(((bf16[512,1408]{1,0:T(8,128)(2,1)}), bf16[2048,1408]{1,0:T(8,128)(2,1)}) %all-gather.13.cloned.1.call-update) | async-done | bytes 5767184 | tf_op jit(solution)/shard_map/all_gather | solution.py:115
  432.2 15.3 %convolution_convert_fusion = bf16[640,2048]{1,0:T(8,128)(2,1)} fusion(bf16[1408,2048]{0,1:T(8,128)(2,1)} %bitcast.75, bf16[2048,1408]{1,0:T(8,128)(2,1)} %all-gather.13.cloned.1.call-done, f32[640,1408]{1,0:T(8,128)} %fusion.14, bf16[640,2048]{1,0:T(8,128)(2,1)S(1)} %copy-done, f32[2048]{0:T(1024)S(1)} %copy-done.3, f32[640]{0:T(1024)S(1)} %add_rsqrt_fusion), kind=kOutput, calls=%fused_computation.13 | convolution fusion | flops 7393935360 | bytes 20392448 | tf_op jit(solution)/shard_map/dot_general | solution.py:122
  447.5 32.8 %reduce-scatter.2.cloned.1.call-done = bf16[640,512]{1,0:T(8,128)(2,1)} async-done(((bf16[640,2048]{1,0:T(8,128)(2,1)}), bf16[640,512]{1,0:T(8,128)(2,1)}) %reduce-scatter.2.cloned.1.call-update) | async-done | bytes 655376 | tf_op jit(solution)/shard_map/reduce_scatter | solution.py:125
  480.2 2.1 add_convert_fusion
  (40 shorter events, 0.8 us)
Async XLA Ops:
  6.5 1.5 copy-start.1
  6.5 76.8 %all-gather.7.cloned.1.call-start = ((), (), s32[]{:S(2)}) async-start(), calls=%async_computation.3 | async-start | bytes 10485760 | tf_op jit(solution)/shard_map/all_gather | solution.py:97
  7.3 12.2 %copy-start.2 = (bf16[640,512]{1,0:T(8,128)(2,1)S(1)}, bf16[640,512]{1,0:T(8,128)(2,1)}, u32[]{:S(2)}) copy-start(bf16[640,512]{1,0:T(8,128)(2,1)} %param.10) | copy-start | bytes 1966084
  7.3 185.0 %all-gather.15.cloned.1.call-start = ((), (), s32[]{:S(2)}) async-start(), calls=%async_computation.8 | async-start | bytes 7208960 | tf_op jit(solution)/shard_map/all_gather | solution.py:120
  9.6 12.9 %collective-permute-start = (bf16[128,2,128]{0,2,1:T(8,128)(2,1)S(1)}, bf16[128,2,128]{0,2,1:T(8,128)(2,1)S(1)}, u32[]{:S(2)}, u32[]{:S(2)}) collective-permute-start(bf16[128,2,128]{0,2,1:T(8,128)(2,1)S(1)} %get-tuple-element.12), channel_id=1, source_target_pairs={{0,4},{4,8},{8,12},{1,5},{5,9},{9,13},{2,6},{6,10},{10,14},{3,7},{... | collective-permute-start | bytes 196616 | tf_op jit(solution)/shard_map/ppermute | solution.py:19
  14.6 8.1 %collective-permute-start.1 = (bf16[128,2,128]{0,2,1:T(8,128)(2,1)S(1)}, bf16[128,2,128]{0,2,1:T(8,128)(2,1)S(1)}, u32[]{:S(2)}, u32[]{:S(2)}) collective-permute-start(bf16[128,2,128]{0,2,1:T(8,128)(2,1)S(1)} %get-tuple-element.11), channel_id=1, source_target_pairs={{4,0},{8,4},{12,8},{5,1},{9,5},{13,9},{6,2},{10,6},{14,10},{7,3},{... | collective-permute-start | bytes 196616 | tf_op jit(solution)/shard_map/ppermute | solution.py:21
  15.9 20.7 %all-to-all-start = ((bf16[4,160,512]{2,1,0:T(8,128)(2,1)}), bf16[4,160,512]{2,1,0:T(8,128)(2,1)S(1)}, u32[]{:S(2)}, u32[]{:S(2)}) async-start(bf16[4,160,512]{2,1,0:T(8,128)(2,1)} %bitcast), calls=%async_computation | async-start | bytes 1310720 | tf_op jit(solution)/shard_map/all_to_all | solution.py:95
  19.7 2.7 copy-start.4
  36.6 21.1 %all-to-all-start.1 = ((bf16[4,160,512]{2,1,0:T(8,128)(2,1)}), bf16[4,160,512]{2,1,0:T(8,128)(2,1)S(1)}, u32[]{:S(2)}, u32[]{:S(2)}) async-start(bf16[4,160,512]{2,1,0:T(8,128)(2,1)} %all_to_all.26), calls=%async_computation.1 | async-start | bytes 1310720 | tf_op jit(solution)/shard_map/all_to_all | solution.py:94
  40.1 177.6 %all-gather.9.cloned.1.call-start = ((), (), s32[]{:S(2)}) async-start(), calls=%async_computation.4 | async-start | bytes 3276800 | tf_op jit(solution)/shard_map/all_gather | solution.py:102
  89.1 236.6 %all-gather.11.cloned.1.call-start = ((), (), s32[]{:S(2)}) async-start(), calls=%async_computation.5 | async-start | bytes 7208960 | tf_op jit(solution)/shard_map/all_gather | solution.py:110
  89.7 342.4 %all-gather.13.cloned.1.call-start = ((), (), s32[]{:S(2)}) async-start(), calls=%async_computation.6 | async-start | bytes 7208960 | tf_op jit(solution)/shard_map/all_gather | solution.py:115
  90.3 389.9 %reduce-scatter.2.cloned.1.call-start = ((), (), s32[]{:S(2)}) async-start(), calls=%async_computation.7 | async-start | bytes 3276800 | tf_op jit(solution)/shard_map/reduce_scatter | solution.py:125
  192.2 133.5 %copy-start.3 = (f32[2048]{0:T(1024)S(1)}, f32[2048]{0:T(1024)}, u32[]{:S(2)}) copy-start(f32[2048]{0:T(1024)} %param.14) | copy-start | bytes 24580
  220.0 212.2 %copy-start = (bf16[640,2048]{1,0:T(8,128)(2,1)S(1)}, bf16[640,2048]{1,0:T(8,128)(2,1)}, u32[]{:S(2)}) copy-start(bf16[640,2048]{1,0:T(8,128)(2,1)} %all-gather.9.cloned.1.call-done) | copy-start | bytes 7864324
Sparse Core Ops, SparseCore 0:
  8.9 74.4 all-gather.6
  84.9 107.2 all-gather.14
  193.8 23.7 all-gather.8
  219.1 106.6 all-gather.10
  327.2 104.9 all-gather.12
  447.6 32.6 reduce-scatter.1
